TPU v7x, 1024 devices: a whole 4x8x16 slice. The times are simulated.
1024 devices in a mesh: sp: 16 (over z), dp: 64 (over y, x, core).
Axes of the slice: x: 4, y: 8, z: 16, core: 2. Of those that a mesh axis runs over, the one named last changes fastest.
Arguments:
- queries: bfloat16 [64, 3072, 1024], P('dp', 'sp'), may hold values from -6 to 6
- keys: bfloat16 [64, 3072, 256], P('dp', 'sp'), may hold values from -6 to 6
- values: bfloat16 [64, 3072, 256], P('dp', 'sp'), may hold values from -6 to 6
- query_gain: float32 [64], replicated, may hold values from 0.15 to 7
- key_gain: float32 [64], replicated, may hold values from 0.15 to 7
- out_weight: bfloat16 [1024, 2048], P(None, 'dp'), may hold values from -0.1875 to 0.1875
- out_gain: float32 [2048], replicated, may hold values from 0.1 to 1.9
Outputs:
- output: bfloat16 [64, 3072, 2048], P('dp', 'sp')
All inputs are finite; a program needn't handle non-finite values.
Results may differ from a plain program's by a relative error of at most 0.0035.
The roundings to bfloat16 on the way count: a program that leaves them out, or rounds other values in their place, can miss the bound.
Values may be sent and summed in bfloat16 or wider, within the bound.
A program may use at most 64 MiB of HBM per device.

v0:
```python
import math

import jax
import jax.numpy as jnp
from jax import lax
from jax.sharding import PartitionSpec as P

QH = 16
KVH = 4
HEAD = 64
GRID_W = 64


EPSILON = 1e-06
ROTARY_BASE = 10000.0


def rotate(vectors, positions, width):
    half_width = width // 2
    frequency = ROTARY_BASE ** (-jnp.arange(0, width, 2, dtype=jnp.float32) / width)
    angles = positions.astype(jnp.float32)[:, None] * frequency[None, :]
    cosines = jnp.cos(angles)[:, None, :]
    sine_table = jnp.sin(angles)[:, None, :]
    first_half = vectors[..., :half_width]
    second_half = vectors[..., half_width:]
    return jnp.concatenate(
        [
            first_half * cosines - second_half * sine_table,
            second_half * cosines + first_half * sine_table,
        ],
        axis=-1,
    )


def prepare(vectors, gain_vector, grid_row, grid_col):
    vectors = vectors.astype(jnp.float32)
    vectors = (
        vectors
        * lax.rsqrt(jnp.mean(vectors * vectors, axis=-1, keepdims=True) + EPSILON)
        * gain_vector
    )
    half_width = HEAD // 2
    turned = jnp.concatenate(
        [
            rotate(vectors[..., :half_width], grid_row, half_width),
            rotate(vectors[..., half_width:], grid_col, half_width),
        ],
        axis=-1,
    )
    return turned.astype(jnp.bfloat16)


def softmax_rows(scores):
    row_max = jnp.max(scores, axis=-1, keepdims=True)
    exponent = jnp.exp(scores - row_max)
    return exponent / jnp.sum(exponent, axis=-1, keepdims=True)


def per_device(queries, keys, values, query_gain, key_gain, out_weight, out_gain):
    sp_count = lax.axis_size("sp")
    tokens_here = queries.shape[1]
    seq_len = tokens_here * sp_count
    score_scale = HEAD ** (-0.5)
    offset = lax.axis_index("sp") * tokens_here
    positions = offset + jnp.arange(tokens_here, dtype=jnp.int32)
    grid_row = positions // GRID_W
    grid_col = positions % GRID_W
    query_rot = prepare(queries[0].reshape(tokens_here, QH, HEAD), query_gain, grid_row, grid_col)
    key_rot = prepare(keys[0].reshape(tokens_here, KVH, HEAD), key_gain, grid_row, grid_col)
    value_heads = values[0].reshape(tokens_here, KVH, HEAD)
    kv_pairs = jnp.concatenate([key_rot, value_heads], axis=2)
    kv_slots = max(KVH, sp_count)
    slot_count = kv_slots // sp_count
    heads_here = QH // sp_count
    per_slot = QH // kv_slots
    copies = jnp.repeat(kv_pairs, kv_slots // KVH, axis=1)
    packed = jnp.concatenate([query_rot, copies], axis=2)
    packed = packed.reshape(tokens_here, sp_count * (heads_here + 2 * slot_count) * HEAD)
    arrived = lax.all_to_all(packed, "sp", split_axis=1, concat_axis=0, tiled=True)
    query_all = arrived[:, : heads_here * HEAD].reshape(seq_len, slot_count, per_slot, HEAD)
    pair_all = arrived[:, heads_here * HEAD :].reshape(seq_len, slot_count, 2, HEAD)
    key_all = pair_all[:, :, 0]
    value_all = pair_all[:, :, 1]
    block_rows = math.gcd(seq_len, 512)

    def attend_block(query_block):
        scores = (
            jnp.einsum("qsrd,ksd->srqk", query_block, key_all, preferred_element_type=jnp.float32)
            * score_scale
        )
        attn_weights = softmax_rows(scores).astype(jnp.bfloat16)
        return jnp.einsum(
            "srqk,ksd->qsrd", attn_weights, value_all, preferred_element_type=jnp.float32
        ).astype(jnp.bfloat16)

    results = lax.map(
        attend_block,
        query_all.reshape(seq_len // block_rows, block_rows, slot_count, per_slot, HEAD),
    )
    heads_out = results.reshape(seq_len, heads_here * HEAD)
    attended = lax.all_to_all(heads_out, "sp", split_axis=0, concat_axis=1, tiled=True)
    projected = jnp.dot(
        attended,
        lax.all_gather(out_weight, "dp", axis=1, tiled=True),
        preferred_element_type=jnp.float32,
    )
    normed = (
        projected
        * lax.rsqrt(jnp.mean(projected * projected, axis=-1, keepdims=True) + EPSILON)
        * out_gain
    )
    return normed.astype(jnp.bfloat16)[None]


def solution(mesh):
    return jax.shard_map(
        per_device,
        mesh=mesh,
        in_specs=(
            P("dp", "sp", None),
            P("dp", "sp", None),
            P("dp", "sp", None),
            P(),
            P(),
            P(None, "dp"),
            P(),
        ),
        out_specs=P("dp", "sp", None),
        check_vma=False,
    )
```

profile of v0, /device:TPU:56, one launch (start us, length us, event | category | flops | bytes accessed | tf_op | source)
XLA Modules:
  0.0 184.9 jit_solution(6868495103581892442)
XLA Ops:
  6.6 1.0 copy.38
  7.6 0.7 fusion.24
  8.7 1.0 copy.39
  9.9 1.2 copy.37
  11.2 0.8 fusion.21
  13.8 1.0 broadcast_in_dim.10
  14.8 5.1 %concatenate.13 = bf16[192,16,192]{2,0,1:T(8,128)(2,1)} concatenate(bf16[192,16,16]{2,0,1:T(8,128)(2,1)S(1)} %copy.41, bf16[192,16,16]{2,0,1:T(8,128)(2,1)S(1)} %copy.42, bf16[192,16,16]{2,0,1:T(8,128)(2,1)S(1)} %copy.43, bf16[192,16,16]{2,0,1:T(8,128)(2,1)S(1)} %copy.44, bf16[192,16,128]{2,0,1:T(8,128)(2,1)} %bitcast.97), dimensions={2} | concatenate | bytes 2359296 | tf_op jit(solution)/shard_map/concatenate | solution.py:77
  20.0 18.9 %all-to-all-start = ((bf16[192,16,192]{2,0,1:T(8,128)(2,1)}), bf16[192,16,192]{2,0,1:T(8,128)(2,1)S(1)}, u32[]{:S(2)}, u32[]{:S(2)}) async-start(bf16[192,16,192]{2,0,1:T(8,128)(2,1)} %concatenate.13), calls=%async_computation | async-start | bytes 3145728 | tf_op jit(solution)/shard_map/all_to_all | solution.py:79
  38.9 0.7 all-gather.2.cloned.1.call-update
  39.6 73.5 %all-to-all-done = bf16[192,16,192]{2,0,1:T(8,128)(2,1)S(1)} async-done(((bf16[192,16,192]{2,0,1:T(8,128)(2,1)}), bf16[192,16,192]{2,0,1:T(8,128)(2,1)S(1)}, u32[]{:S(2)}, u32[]{:S(2)}) %all-to-all-start) | async-done | bytes 1179680 | tf_op jit(solution)/shard_map/all_to_all | solution.py:79
  114.1 23.0 %while.10 = (s32[]{:T(128)}, bf16[6,512,1,1,64]{1,4,3,2,0:T(8,128)(2,1)S(1)}, bf16[6,512,1,1,64]{1,4,3,2,0:T(8,128)(2,1)S(1)}, bf16[3072,1,64]{0,2,1:T(8,128)(2,...) while((s32[]{:T(128)}, bf16[6,512,1,1,64]{1,4,3,2,0:T(8,128)(2,1)S(1)}, ...), condition=%wide.region_5.6_spmd, body=%wide.region_2.5_spmd.sunk | while | flops 416840704 | bytes 19802188 | solution.py:96
  114.1 1.1 multiply_reduce_fusion.3
  115.2 1.2 fusion.40
  116.3 1.6 fusion.41
  117.9 1.1 multiply_reduce_fusion.3
  119.0 1.2 fusion.40
  120.2 1.6 fusion.41
  121.8 1.1 multiply_reduce_fusion.3
  122.9 1.2 fusion.40
  124.0 1.6 fusion.41
  125.6 1.1 multiply_reduce_fusion.3
  126.7 1.2 fusion.40
  127.9 1.6 fusion.41
  129.4 1.1 multiply_reduce_fusion.3
  130.5 1.2 fusion.40
  131.7 1.6 fusion.41
  133.3 1.1 multiply_reduce_fusion.3
  134.4 1.2 fusion.40
  135.5 1.6 fusion.41
  138.1 35.0 %all_to_all.35 = bf16[16,192,64]{1,2,0:T(8,128)(2,1)S(1)} all-to-all(bf16[16,192,64]{1,2,0:T(8,128)(2,1)S(1)} %copy.49), channel_id=1, replica_groups=mesh['sp'=16,'dp'=64] {'sp'}, dimensions={0} | all-to-all | bytes 786432 | tf_op jit(solution)/shard_map/all_to_all | solution.py:101
  173.2 3.8 %multiply_reduce_fusion.1 = (f32[192]{0:T(256)S(1)}, f32[192,2048]{1,0:T(8,128)S(1)}) fusion(bf16[192,1024]{0,1:T(8,128)(2,1)S(1)} %bitcast.98, bf16[1024,2048]{0,1:T(8,128)(2,1)} %all-gather.2.cloned.1.call-done), kind=kOutput, calls=%fused_computation.18 | convolution fusion | flops 806092608 | bytes 6161152 | tf_op jit(solution)/shard_map/dot_general | solution.py:102
  177.0 1.1 fusion.22
  (32 shorter events, 4.4 us)
Async XLA Ops:
  20.0 93.1 %all-to-all-start = ((bf16[192,16,192]{2,0,1:T(8,128)(2,1)}), bf16[192,16,192]{2,0,1:T(8,128)(2,1)S(1)}, u32[]{:S(2)}, u32[]{:S(2)}) async-start(bf16[192,16,192]{2,0,1:T(8,128)(2,1)} %concatenate.13), calls=%async_computation | async-start | bytes 3145728 | tf_op jit(solution)/shard_map/all_to_all | solution.py:79
  38.9 134.3 %all-gather.2.cloned.1.call-start = ((), (), s32[]{:S(2)}) async-start(), calls=%async_computation.2 | async-start | bytes 4259840 | tf_op jit(solution)/shard_map/all_gather | solution.py:104
  137.1 39.9 %copy-start = (f32[2048]{0:T(1024)S(1)}, f32[2048]{0:T(1024)}, u32[]{:S(2)}) copy-start(f32[2048]{0:T(1024)} %param.15) | copy-start | bytes 24580
Sparse Core Ops, SparseCore 0:
  44.2 94.5 all-gather.1
where the time goes:
time: 185 us
  waiting for transfers between devices  74.2 us (40%)
  blocking collectives  35 us (19%)
  matrix products  19.7 us (11%)
  starting transfers between devices  18.9 us (10%)
  between operations  13.6 us (7%)
  local copies, waits for them, and re-layouts  13 us (7%)
  other arithmetic  10.3 us (6%)
    all_to_all x1, waiting for transfers between devices, per_device(): lax.all_to_all(packed, 'sp', split_axis=1, concat_axis=0, tiled=True)  73.5 us
    all_to_all x1, blocking collectives, per_device(): lax.all_to_all(heads_out, 'sp', split_axis=0, concat_axis=1, tiled=True)  35 us
    all_to_all x1, starting transfers between devices, per_device(): lax.all_to_all(packed, 'sp', split_axis=1, concat_axis=0, tiled=True)  18.9 us
    dot_general x6, matrix products, attend_block(): jnp.einsum('srqk,ksd->qsrd', attn_weights, value_all, preferred_element_t...  9.34 us
    reduce_sum x6, other arithmetic, softmax_rows(): return exponent / jnp.sum(exponent, axis=-1, keepdims=True)  7 us
    dot_general x6, matrix products, attend_block(): jnp.einsum('qsrd,ksd->srqk', query_block, key_all, preferred_element_type...  6.56 us
    concatenate x1, local copies, waits for them, and re-layouts, per_device(): packed = jnp.concatenate([query_rot, copies], axis=2)  5.14 us
    dot_general x1, matrix products, per_device(): jnp.dot(attended, lax.all_gather(out_weight, 'dp', axis=1, tiled=True), p...  3.78 us
  transfers between devices with their start and end apart: 2, of which 1 were waited for; matrix products, arithmetic and copies ran while one was open for 13% of the time, Pallas kernels for 0%

commit v1 on v0

v1 whole, which is shorter than its diff:
```python
import functools
import math

import jax
import jax.numpy as jnp
import numpy as np
from jax import lax
from jax.experimental import pallas as pl
from jax.experimental.pallas import tpu as pltpu
from jax.sharding import PartitionSpec as P

MESH = pl.DeviceIdType.MESH
F32 = jnp.float32
BF16 = jnp.bfloat16
NZ = 16
NX, NY = 4, 8
TOK = 192
LOG2E = math.log2(math.e)
EPS = 1e-06
MID = 10
SLOTS = 21
NC = 2
LAG = 1
TICKS = 9
WTICKS = 20


def tables():
    freq = (10000.0 ** (-(np.arange(0, 32, 2, dtype=np.float32) / np.float32(32)))).astype(np.float32)
    lane = np.arange(256)
    is_row = lane % 64 < 32
    first = lane % 32 < 16
    sign = np.where(first, -1.0, 1.0)
    by_lane = freq[lane % 16]
    row_angle = (np.arange(48, dtype=np.float32)[:, None] * by_lane[None]).astype(np.float64)
    col_angle = (np.arange(64, dtype=np.float32)[:, None] * by_lane[None]).astype(np.float64)
    row_tab = np.zeros((NZ, 2, 8, 256), np.float32)
    row_tab[:, 0, :3] = np.where(is_row, np.cos(row_angle), 0).reshape(NZ, 3, 256)
    row_tab[:, 1, :3] = np.where(is_row, np.sin(row_angle) * sign, 0).reshape(NZ, 3, 256)
    col_tab = np.stack([np.where(is_row, 0, np.cos(col_angle)), np.where(is_row, 0, np.sin(col_angle) * sign)])
    partner = np.where(first, lane + 16, lane - 16)
    mats = np.zeros((2, 256, 256), np.float32)
    mats[0, partner, lane] = 1
    mats[1] = (lane[:, None] // 64 == lane[None] // 64) / 64.0
    return row_tab, col_tab.astype(np.float32), mats.astype(jnp.bfloat16)


def n_right(z):
    one = lambda c: jnp.where(c, 1, 0).astype(jnp.int32)
    return 6 + one(z >= 2) + one(z >= 4) - one(z >= 9)


def delay(z):
    one = lambda c: jnp.where(c, 1, 0).astype(jnp.int32)
    return 3 - one(z >= 2) - one(z >= 4) - one(z >= 5)


def gain_rows(gain):
    two = jnp.broadcast_to(jnp.concatenate([gain, gain], axis=1), (8, 128))
    lane = lax.broadcasted_iota(jnp.int32, (8, 128), 1)
    swapped = jnp.where(lane % 32 < 16, pltpu.roll(two, 112, 1), pltpu.roll(two, 16, 1))
    wide = lambda a: jnp.concatenate([a, a], axis=1)[0:1]
    return wide(two), wide(swapped)


def rope(x, gain, row_tab, col_tab, mats):
    g, gp = gain
    xf = x.astype(F32)
    sq = xf * xf
    hi = sq.astype(BF16)
    lo = (sq - hi.astype(F32)).astype(BF16)
    mean = jnp.dot(hi, mats[1], preferred_element_type=F32) + jnp.dot(lo, mats[1], preferred_element_type=F32)
    xp = jnp.dot(x, mats[0], preferred_element_type=F32)
    r = lax.rsqrt(mean + EPS)
    parts = []
    for i in range(3):
        rows = slice(64 * i, 64 * i + 64)
        c = (col_tab[0] + row_tab[0, i : i + 1, :]) * g
        s = (col_tab[1] + row_tab[1, i : i + 1, :]) * gp
        parts.append((xf[rows] * c + xp[rows] * s) * r[rows])
    return jnp.concatenate(parts, axis=0)


def kernel(
    q_hbm, k_hbm, v_hbm, w_hbm, qg_ref, kg_ref, og_ref, row_hbm, col_hbm, mats_hbm,
    out_ref,
    qb, kraw, wraw, row_tab, col_tab, mats,
    KB, VB, VT, WB, QX, KX, M, L, MB, E, OT, ATT, PROJ,
    in_sem, ks_sem, kr_sem, vs_sem, vr_sem, wx_ss, wx_rs, wy_ss, wy_rs, wd_ss, wd_rs,
):
    z = lax.axis_index("sp")
    d = lax.axis_index("dp")
    core = d % 2
    x = (d // 2) % NX
    y = d // (2 * NX)
    up, down = (z + 1) % NZ, (z + NZ - 1) % NZ
    at = lambda xx, yy, cc: (z, (yy * NX + xx) * 2 + cc)
    nR = n_right(z)
    nL = (NZ - 1) - nR
    low = MID - nR

    loads = [
        pltpu.make_async_copy(k_hbm.at[0], kraw, in_sem.at[0]),
        pltpu.make_async_copy(row_hbm.at[z], row_tab, in_sem.at[1]),
        pltpu.make_async_copy(col_hbm, col_tab, in_sem.at[2]),
        pltpu.make_async_copy(mats_hbm, mats, in_sem.at[3]),
        pltpu.make_async_copy(v_hbm.at[0], VB.at[MID], in_sem.at[4]),
        pltpu.make_async_copy(w_hbm, wraw, in_sem.at[5]),
        pltpu.make_async_copy(q_hbm.at[0], qb, in_sem.at[6]),
    ]
    for c in loads:
        c.start()

    barrier = pltpu.get_barrier_semaphore()
    sib = at(x, y, 1 - core)
    partners = [
        (up, d), (down, d),
        at((x + 1) % NX, y, core), at((x + 2) % NX, y, core), at((x + 3) % NX, y, core),
        at(x, (y + 1) % NY, core), at(x, (y + NY - 1) % NY, core), sib,
    ]
    for p in partners:
        pl.semaphore_signal(barrier, inc=1, device_id=p, device_id_type=MESH)

    for c in loads[:4]:
        c.wait()
    kg = gain_rows(kg_ref[...])
    KB[MID] = rope(kraw[...], kg, row_tab, col_tab, mats).astype(BF16)
    loads[4].wait()
    loads[5].wait()
    eye = (lax.broadcasted_iota(jnp.int32, (32, 32), 0) == lax.broadcasted_iota(jnp.int32, (32, 32), 1)).astype(BF16)
    own_w = lax.dot_general(eye, wraw[...], (((1,), (1,)), ((), ())), preferred_element_type=F32)
    WB[d] = own_w.astype(BF16)
    pl.semaphore_wait(barrier, len(partners))

    def kv(buf, ss, rs, b, sg, c):
        rows = pl.ds(c * (TOK // NC), TOK // NC)
        return pltpu.make_async_remote_copy(
            src_ref=buf.at[b, rows], dst_ref=buf.at[b + sg, rows], send_sem=ss.at[b + sg, c],
            recv_sem=rs.at[b + sg, c], device_id=((z - sg + NZ) % NZ, d), device_id_type=MESH,
        )

    def own(buf, ss, rs):
        for c in range(NC):
            for sg in (-1, 1):
                kv(buf, ss, rs, MID, sg, c).start()

    def arrive(buf, ss, rs, sg, k):
        b = MID + sg * k
        there = (z - sg + NZ) % NZ
        most = jnp.where(sg < 0, n_right(there), (NZ - 1) - n_right(there))
        for c in range(NC):
            kv(buf, ss, rs, b - sg, sg, c).wait_recv()

            @pl.when(k + 1 <= most)
            def _():
                kv(buf, ss, rs, b, sg, c).start()

    def sent(buf, ss, rs, sg, k):
        there = (z - sg + NZ) % NZ
        most = jnp.where(sg < 0, n_right(there), (NZ - 1) - n_right(there))

        @pl.when(k + 1 <= most)
        def _():
            for c in range(NC):
                kv(buf, ss, rs, MID + sg * k, sg, c).wait_send()

    own(KB, ks_sem, kr_sem)
    own(VB, vs_sem, vr_sem)

    def wx(j):
        return pltpu.make_async_remote_copy(
            src_ref=WB.at[d], dst_ref=WB.at[d], send_sem=wx_ss.at[j], recv_sem=wx_rs.at[j],
            device_id=at((x + NX - j) % NX, y, core), device_id_type=MESH,
        )

    def wblock(j, s):
        return (((y + NY - s) % NY) * NX + (x + j) % NX) * 2 + core

    def wy(j, s, sg):
        blk = wblock(j, NY - sg * s if not isinstance(s, int) else (-sg * s) % NY)
        return pltpu.make_async_remote_copy(
            src_ref=WB.at[blk], dst_ref=WB.at[blk], send_sem=wy_ss.at[(sg + 1) // 2, j, s + 1],
            recv_sem=wy_rs.at[(sg + 1) // 2, j, s + 1],
            device_id=at(x, (y - sg + NY) % NY, core), device_id_type=MESH,
        )

    def wd(blk):
        return pltpu.make_async_remote_copy(
            src_ref=WB.at[blk], dst_ref=WB.at[blk], send_sem=wd_ss.at[blk // 2], recv_sem=wd_rs.at[blk // 2],
            device_id=sib, device_id_type=MESH,
        )

    for j in (1, 2, 3):
        wx(j).start()
    wd(d).start()

    def w_side(j, s, sg, upto):
        most = upto(j, sg)
        blk = wblock(j, NY - sg * s)

        @pl.when(s <= most)
        def _():
            wy(j, s - 1, sg).wait_recv()
            wd(blk).start()

        @pl.when(s + 1 <= most)
        def _():
            wy(j, s, sg).start()

    def upto(j, sg):
        even = jnp.where(j % 2 == 0, 1, 0)
        return jnp.where(sg < 0, 3 + even, 4 - even)

    def w_tick(i):
        s, j = i // 4, i % 4

        @pl.when(s == 0)
        def _():
            @pl.when(j > 0)
            def _():
                wx(j).wait_recv()
                wd(wblock(j, 0)).start()

            wy(j, s, -1).start()
            wy(j, s, 1).start()

        @pl.when(s > 0)
        def _():
            w_side(j, s, -1, upto)
            w_side(j, s, 1, upto)

    loads[6].wait()
    qg = gain_rows(qg_ref[...])
    lane = lax.broadcasted_iota(jnp.int32, (64, 128), 1)

    def put(t, half, val):
        hi = val.astype(BF16)
        rest = val - hi.astype(F32)
        mid = rest.astype(BF16)
        lo = (rest - mid.astype(F32)).astype(BF16)
        cols = slice(128 * half, 128 * half + 128)
        QX[t, 0:64, cols] = hi
        QX[t, 64:128, cols] = mid
        QX[t, 128:192, cols] = lo
        QX[t, 192:256, cols] = jnp.zeros((64, 128), BF16)

    for g in range(4):
        qr = rope(qb[:, 256 * g : 256 * g + 256], qg, row_tab, col_tab, mats)
        qr = qr.astype(BF16).astype(F32) * (0.125 * LOG2E)
        a = jnp.transpose(qr[0:128])
        b = jnp.transpose(jnp.concatenate([qr[128:192], jnp.zeros((64, 256), F32)], axis=0))
        for r in range(4):
            put(3 * g + r // 2, r % 2, a[64 * r : 64 * r + 64])
        for h in range(2):
            b0, b1 = b[128 * h : 128 * h + 64], pltpu.roll(b[128 * h + 64 : 128 * h + 128], 64, 1)
            put(3 * g + 2, h, jnp.where(lane < 64, b0, b1))
    M[...] = jnp.full_like(M, -1e30)
    L[...] = jnp.zeros_like(L)
    OT[...] = jnp.zeros_like(OT)
    lane2 = lax.broadcasted_iota(jnp.int32, (TOK, 128), 1)

    def pass1(b):
        for pr in range(2):
            v = KB[b, :, 128 * pr : 128 * pr + 128].astype(F32)
            rt = pltpu.roll(v, 64, 1)
            for o in range(2):
                dup = jnp.where(lane2 < 64, v, rt) if o == 0 else jnp.where(lane2 < 64, rt, v)
                dup = dup.astype(BF16)
                KX[2 * pr + o, :, 0:128] = dup
                KX[2 * pr + o, :, 128:256] = dup
        i = b - low
        for t in range(12):
            s = jnp.dot(KX[t // 3], QX[t], preferred_element_type=F32).reshape(TOK // 8, 8, 256)
            old = M[t]
            new = jnp.maximum(old, jnp.max(s, axis=0))
            e = jnp.exp2(s - new[None])
            L[t] = L[t] * jnp.exp2(old - new) + jnp.sum(e, axis=0)
            M[t] = new
            MB[i, t] = new
            E[i, t] = e.reshape(TOK, 256)

    def turn_v(b):
        v = VB[b].astype(F32)
        i = b - low
        VT[i, :, 0:128] = jnp.transpose(v[0:128]).astype(BF16)
        VT[i, :, 128:256] = jnp.transpose(jnp.concatenate([v[128:192], jnp.zeros((64, 256), F32)], axis=0)).astype(BF16)

    def pass2(i):
        for t in range(12):
            g = t // 3
            f = jnp.exp2(MB[i, t] - M[t])
            p = (E[i, t].reshape(TOK // 8, 8, 256) * f[None]).reshape(TOK, 256).astype(BF16)
            OT[t] += jnp.dot(VT[i, 64 * g : 64 * g + 64, 0:TOK], p, preferred_element_type=F32)

    pass1(MID)
    turn_v(MID)
    late = delay(z)

    def tick(t, carry):
        def side(j, c2):
            sg = 1 - 2 * j
            k_plain = t + 1
            k_late = t + 1 - late
            k = jnp.where((sg > 0) | (k_plain <= z), k_plain, k_late)
            ok = jnp.where(sg > 0, k <= nL, (k <= nR) & ((k_plain <= z) | (k_late > z)))

            @pl.when(ok)
            def _():
                arrive(KB, ks_sem, kr_sem, sg, k)

                @pl.when(k > LAG)
                def _():
                    arrive(VB, vs_sem, vr_sem, sg, k - LAG)
                    turn_v(MID + sg * (k - LAG))

                pass1(MID + sg * k)

            @pl.when(2 * t + j < WTICKS)
            def _():
                w_tick(2 * t + j)

            return c2

        return lax.fori_loop(0, 2, side, carry)

    lax.fori_loop(0, TICKS, tick, 0)

    def w_more(i, c):
        w_tick(i)
        return c

    lax.fori_loop(2 * TICKS, WTICKS, w_more, 0)

    m = M[...]
    top = jnp.max(m, axis=1, keepdims=True)
    total = jnp.sum(L[...] * jnp.exp2(m - top), axis=1, keepdims=True)
    M[...] = jnp.broadcast_to(top + jnp.log(total) * LOG2E, M.shape)

    for sg, n in ((1, nL), (-1, nR)):
        for back in range(LAG):
            k = n - LAG + 1 + back
            arrive(VB, vs_sem, vr_sem, sg, k)
            turn_v(MID + sg * k)

    def p2(i, c):
        pass2(i)
        return c

    lax.fori_loop(0, NZ, p2, 0)

    for g in range(4):
        for p in range(2):
            a = jnp.concatenate([OT[3 * g + p, :, 0:128], OT[3 * g + p, :, 128:256]], axis=0)
            ATT[0:128, 256 * g + 128 * p : 256 * g + 128 * p + 128] = jnp.transpose(a).astype(BF16)
            b = OT[3 * g + 2, :, 128 * p : 128 * p + 128]
            b = jnp.transpose(jnp.concatenate([b, b], axis=0))
            ATT[128:192, 256 * g + 128 * p : 256 * g + 128 * p + 128] = jnp.where(lane < 64, b[0:64], b[64:128]).astype(BF16)

    def w_in(i, c):
        wd(2 * i + 1 - core).wait_recv()
        return c

    lax.fori_loop(0, NX * NY, w_in, 0)

    def project(n, ss):
        w = WB[pl.ds(8 * n, 8)].reshape(256, 1024)
        pr = lax.dot_general(ATT[...], w, (((1,), (1,)), ((), ())), preferred_element_type=F32)
        PROJ[n] = pr
        sq = pr * pr
        return ss + sq[:, 0:128] + sq[:, 128:256]

    ss = lax.fori_loop(0, 8, project, jnp.zeros((TOK, 128), F32))
    r = lax.rsqrt(jnp.sum(ss, axis=1, keepdims=True) / 2048.0 + EPS)
    for n in range(8):
        cols = slice(256 * n, 256 * n + 256)
        out_ref[0, :, cols] = (PROJ[n] * r * og_ref[:, cols]).astype(BF16)

    def out_kv(k, c):
        for sg in (-1, 1):
            sent(KB, ks_sem, kr_sem, sg, k)
            sent(VB, vs_sem, vr_sem, sg, k)
        return c

    lax.fori_loop(0, 10, out_kv, 0)
    for j in (1, 2, 3):
        wx(j).wait_send()

    def out_w(i, c):
        s, j = i // 4, i % 4
        for sg in (-1, 1):

            @pl.when(s + 1 <= upto(j, sg))
            def _():
                wy(j, s, sg).wait_send()

        return c

    lax.fori_loop(0, 16, out_w, 0)

    def out_d(i, c):
        wd(2 * i + core).wait_send()
        return c

    lax.fori_loop(0, NX * NY, out_d, 0)


def per_device(queries, keys, values, query_gain, key_gain, out_weight, out_gain):
    row_tab, col_tab, mats = tables()
    hbm = pl.BlockSpec(memory_space=pl.ANY)
    vmem = pl.BlockSpec(memory_space=pltpu.VMEM)
    dma = pltpu.SemaphoreType.DMA
    return pl.pallas_call(
        kernel,
        out_shape=jax.ShapeDtypeStruct((1, TOK, 2048), BF16),
        in_specs=[hbm, hbm, hbm, hbm, vmem, vmem, vmem, hbm, hbm, hbm],
        out_specs=vmem,
        scratch_shapes=[
            pltpu.VMEM((TOK, 1024), BF16), pltpu.VMEM((TOK, 256), BF16), pltpu.VMEM((1024, 32), BF16),
            pltpu.VMEM((2, 8, 256), F32), pltpu.VMEM((2, 64, 256), F32), pltpu.VMEM((2, 256, 256), BF16),
            pltpu.VMEM((SLOTS, TOK, 256), BF16), pltpu.VMEM((SLOTS, TOK, 256), BF16), pltpu.VMEM((NZ, 256, 256), BF16),
            pltpu.VMEM((64, 32, 1024), BF16), pltpu.VMEM((12, 256, 256), BF16), pltpu.VMEM((4, TOK, 256), BF16),
            pltpu.VMEM((12, 8, 256), F32), pltpu.VMEM((12, 8, 256), F32), pltpu.VMEM((NZ, 12, 8, 256), F32),
            pltpu.VMEM((NZ, 12, TOK, 256), F32), pltpu.VMEM((12, 64, 256), F32), pltpu.VMEM((TOK, 1024), BF16),
            pltpu.VMEM((8, TOK, 256), F32),
            dma((7,)), dma((SLOTS, NC)), dma((SLOTS, NC)), dma((SLOTS, NC)), dma((SLOTS, NC)),
            dma((4,)), dma((4,)), dma((2, 4, 5)), dma((2, 4, 5)), dma((32,)), dma((32,)),
        ],
        compiler_params=pltpu.CompilerParams(
            collective_id=0, has_side_effects=True, vmem_limit_bytes=67043328
        ),
        name="attend",
    )(
        queries, keys, values, out_weight, query_gain[None], key_gain[None], out_gain[None],
        jnp.asarray(row_tab), jnp.asarray(col_tab), jnp.asarray(mats),
    )


def solution(mesh):
    return jax.shard_map(
        per_device,
        mesh=mesh,
        in_specs=(
            P("dp", "sp", None),
            P("dp", "sp", None),
            P("dp", "sp", None),
            P(),
            P(),
            P(None, "dp"),
            P(),
        ),
        out_specs=P("dp", "sp", None),
        check_vma=False,
    )
```

time: 185 us -> 90.9 us (0.49)
  the two profiles are of different devices: /device:TPU:56 before, /device:TPU:272 now
where the time goes in v1:
time: 90.9 us; the launch traced here: 90.6 us
  Pallas kernels  86.8 us (95%)
  local copies, waits for them, and re-layouts  3.77 us (4%)
    pallas_call x1, Pallas kernels, per_device(): pl.pallas_call(kernel, out_shape=jax.ShapeDtypeStruct((1, TOK, 2048), BF1...  86.8 us
    unnamed x2, local copies, waits for them, and re-layouts  3.77 us

profile of v1, /device:TPU:272, one launch (start us, length us, event | category | flops | bytes accessed | tf_op | source)
XLA Modules:
  0.0 90.6 jit_solution(2215613549400577573)
XLA Ops:
  0.0 1.7 %copy.11.w_hbm = bf16[1024,32]{1,0:T(8,128)(2,1)} copy(bf16[1024,32]{0,1:T(8,128)(2,1)} %param.15) | data formatting | bytes 131072 | tf_op args[5]
  1.7 86.8 %attend.1 = bf16[1,192,2048]{2,1,0:T(8,128)(2,1)} custom-call(bf16[1,192,1024]{2,1,0:T(8,128)(2,1)} %q_hbm.1, bf16[1,192,256]{2,1,0:T(8,128)(2,1)} %k_hbm.1, bf16[1,192,256]{2,1,0:T(8,128)(2,1)} %v_hbm.1, bf16[1024,32]{1,0:T(8,128)(2,1)} %copy.11.w_hbm, f32[1,64]{1,0:T(1,128)} %bitcast.4, f32[1,64]{1,0:T(1,128)} %bitcast.5, f32[1,2048]{1,0:T(1,128)} %bitcast.3, ...), custom_call_target="tpu_custom_call" | custom-call | tf_op jit(solution)/shard_map/attend/pallas_call | solution.py:412
  88.5 2.1 %copy.13 = bf16[1,192,2048]{2,1,0:T(8,128)(2,1)} copy(bf16[1,192,2048]{2,1,0:T(8,128)(2,1)} %attend.1) | data formatting | bytes 1572864

commit v2 on v1

--- a/solution.py
+++ b/solution.py
@@ -20,9 +20,20 @@
 MID = 10
 SLOTS = 21
 NC = 2
-LAG = 1
-TICKS = 9
 WTICKS = 20
+N_RIGHT = (7, 7, 7, 7, 7, 7, 7, 7, 7, 7, 7, 7, 7, 7, 7, 7)
+ORDER = (
+    (328470619, 293635227, 170919067, 293635227, 293635227, 696288411, 176424091, 293635227, 621024411, 621024411, 621024411, 621024411, 621024411, 621024411, 621024411, 696288411),
+    (327320203, 192190165, 290326058, 170930389, 170930389, 170930386, 170930389, 170930389, 696288922, 696288922, 696288922, 696288922, 696288922, 696288922, 696288915, 621024467),
+    (327320203, 696289001, 192190185, 290326058, 290326058, 290326058, 290326058, 170930410, 696288922, 696288922, 696288922, 696288922, 696288922, 696288922, 696288915, 621024467),
+    (327323731, 696288922, 290308137, 410293993, 174702913, 174702913, 290326337, 170930410, 696288922, 696288922, 696288922, 696288922, 696288922, 696288922, 696288915, 621024467),
+    (327323731, 170930386, 172867625, 409637984, 547624681, 172898824, 290326337, 170930410, 696288922, 696288922, 696288922, 696288922, 696288922, 696288922, 696288915, 621024467),
+    (327323731, 290326037, 174702920, 409555552, 51684051, 696289001, 290326337, 170930410, 696288922, 696288922, 696288922, 696288922, 696288922, 696288922, 696288915, 621024467),
+    (694325913, 290326057, 40487432, 409637984, 409637980, 547624147, 691024105, 290326338, 170930330, 696288922, 696288922, 696288922, 696288922, 696288922, 696288915, 621024467),
+    (1055471384, 376029505, 860705537, 508469856, 510301280, 1047831195, 1047828122, 1047828201, 1047828181, 1047828122, 1047828122, 1047828122, 1047828122, 1047828122, 1047828115, 930387155),
+    (1056698302, 937393663, 937394167, 1056701943, 1056931319, 1071611379, 937393651, 937393651, 937393651, 937393651, 937393651, 937393651, 937393651, 937393651, 937393651, 1056698299),
+    (920350135, 920350199, 920350647, 920350654, 920350654, 920350654, 920350711, 920350711, 920350711, 920350711, 920350711, 920350711, 920350711, 920350711, 920350711, 920350654),
+)
 
 
 def tables():
@@ -45,14 +56,12 @@
     return row_tab, col_tab.astype(np.float32), mats.astype(jnp.bfloat16)
 
 
-def n_right(z):
-    one = lambda c: jnp.where(c, 1, 0).astype(jnp.int32)
-    return 6 + one(z >= 2) + one(z >= 4) - one(z >= 9)
-
-
-def delay(z):
-    one = lambda c: jnp.where(c, 1, 0).astype(jnp.int32)
-    return 3 - one(z >= 2) - one(z >= 4) - one(z >= 5)
+def pick(values, z):
+    out = jnp.int32(values[0])
+    for i, v in enumerate(values[1:], 1):
+        if v != values[0]:
+            out = jnp.where(z == i, jnp.int32(v), out)
+    return out
 
 
 def gain_rows(gain):
@@ -84,18 +93,18 @@
 def kernel(
     q_hbm, k_hbm, v_hbm, w_hbm, qg_ref, kg_ref, og_ref, row_hbm, col_hbm, mats_hbm,
     out_ref,
-    qb, kraw, wraw, row_tab, col_tab, mats,
-    KB, VB, VT, WB, QX, KX, M, L, MB, E, OT, ATT, PROJ,
-    in_sem, ks_sem, kr_sem, vs_sem, vr_sem, wx_ss, wx_rs, wy_ss, wy_rs, wd_ss, wd_rs,
+    qb, kraw, row_tab, col_tab, mats,
+    KV, VT, WB, QX, KX, M, L, MB, E, OT, ATT, PROJ,
+    in_sem, s_sem, r_sem, wx_ss, wx_rs, wy_ss, wy_rs, wd_ss, wd_rs, late_sem,
 ):
     z = lax.axis_index("sp")
     d = lax.axis_index("dp")
-    core = d % 2
-    x = (d // 2) % NX
-    y = d // (2 * NX)
-    up, down = (z + 1) % NZ, (z + NZ - 1) % NZ
+    core = d & 1
+    x = (d >> 1) & (NX - 1)
+    y = d >> 3
+    up, down = (z + 1) & (NZ - 1), (z - 1) & (NZ - 1)
     at = lambda xx, yy, cc: (z, (yy * NX + xx) * 2 + cc)
-    nR = n_right(z)
+    nR = pick(N_RIGHT, z)
     nL = (NZ - 1) - nR
     low = MID - nR
 
@@ -104,8 +113,8 @@
         pltpu.make_async_copy(row_hbm.at[z], row_tab, in_sem.at[1]),
         pltpu.make_async_copy(col_hbm, col_tab, in_sem.at[2]),
         pltpu.make_async_copy(mats_hbm, mats, in_sem.at[3]),
-        pltpu.make_async_copy(v_hbm.at[0], VB.at[MID], in_sem.at[4]),
-        pltpu.make_async_copy(w_hbm, wraw, in_sem.at[5]),
+        pltpu.make_async_copy(v_hbm.at[0], KV.at[MID + SLOTS], in_sem.at[4]),
+        pltpu.make_async_copy(w_hbm, WB.at[d], in_sem.at[5]),
         pltpu.make_async_copy(q_hbm.at[0], qb, in_sem.at[6]),
     ]
     for c in loads:
@@ -114,79 +123,72 @@
     barrier = pltpu.get_barrier_semaphore()
     sib = at(x, y, 1 - core)
     partners = [
-        (up, d), (down, d),
-        at((x + 1) % NX, y, core), at((x + 2) % NX, y, core), at((x + 3) % NX, y, core),
-        at(x, (y + 1) % NY, core), at(x, (y + NY - 1) % NY, core), sib,
+        (down, d),
+        at((x + 1) & (NX - 1), y, core), at((x + 2) & (NX - 1), y, core), at((x + 3) & (NX - 1), y, core),
+        at(x, (y + 1) & (NY - 1), core), at(x, (y - 1) & (NY - 1), core), sib,
     ]
     for p in partners:
         pl.semaphore_signal(barrier, inc=1, device_id=p, device_id_type=MESH)
 
+    @pl.when(z != NZ - 1)
+    def _():
+        pl.semaphore_signal(barrier, inc=1, device_id=(up, d), device_id_type=MESH)
+
     for c in loads[:4]:
         c.wait()
     kg = gain_rows(kg_ref[...])
-    KB[MID] = rope(kraw[...], kg, row_tab, col_tab, mats).astype(BF16)
+    KV[MID] = rope(kraw[...], kg, row_tab, col_tab, mats).astype(BF16)
     loads[4].wait()
     loads[5].wait()
-    eye = (lax.broadcasted_iota(jnp.int32, (32, 32), 0) == lax.broadcasted_iota(jnp.int32, (32, 32), 1)).astype(BF16)
-    own_w = lax.dot_general(eye, wraw[...], (((1,), (1,)), ((), ())), preferred_element_type=F32)
-    WB[d] = own_w.astype(BF16)
-    pl.semaphore_wait(barrier, len(partners))
-
-    def kv(buf, ss, rs, b, sg, c):
+    pl.semaphore_wait(barrier, len(partners) + jnp.where(z == 0, 0, 1))
+
+    @pl.when(z == NZ - 1)
+    def _():
+        pl.semaphore_signal(late_sem, inc=1, device_id=(0, d), device_id_type=MESH)
+
+    there = lambda sg: jnp.where(sg < 0, up, down)
+
+    def kv(b, sg, c):
         rows = pl.ds(c * (TOK // NC), TOK // NC)
         return pltpu.make_async_remote_copy(
-            src_ref=buf.at[b, rows], dst_ref=buf.at[b + sg, rows], send_sem=ss.at[b + sg, c],
-            recv_sem=rs.at[b + sg, c], device_id=((z - sg + NZ) % NZ, d), device_id_type=MESH,
+            src_ref=KV.at[b, rows], dst_ref=KV.at[b + sg, rows], send_sem=s_sem.at[b + sg, c],
+            recv_sem=r_sem.at[b + sg, c], device_id=(there(sg), d), device_id_type=MESH,
         )
 
-    def own(buf, ss, rs):
+    def own(b, sg):
         for c in range(NC):
-            for sg in (-1, 1):
-                kv(buf, ss, rs, MID, sg, c).start()
-
-    def arrive(buf, ss, rs, sg, k):
-        b = MID + sg * k
-        there = (z - sg + NZ) % NZ
-        most = jnp.where(sg < 0, n_right(there), (NZ - 1) - n_right(there))
-        for c in range(NC):
-            kv(buf, ss, rs, b - sg, sg, c).wait_recv()
-
-            @pl.when(k + 1 <= most)
-            def _():
-                kv(buf, ss, rs, b, sg, c).start()
-
-    def sent(buf, ss, rs, sg, k):
-        there = (z - sg + NZ) % NZ
-        most = jnp.where(sg < 0, n_right(there), (NZ - 1) - n_right(there))
-
-        @pl.when(k + 1 <= most)
-        def _():
-            for c in range(NC):
-                kv(buf, ss, rs, MID + sg * k, sg, c).wait_send()
-
-    own(KB, ks_sem, kr_sem)
-    own(VB, vs_sem, vr_sem)
+            kv(b, sg, c).start()
+
+    own(MID, -1)
+
+    @pl.when(z == 0)
+    def _():
+        own(MID + SLOTS, -1)
+
+    @pl.when(z != 0)
+    def _():
+        own(MID, 1)
 
     def wx(j):
         return pltpu.make_async_remote_copy(
             src_ref=WB.at[d], dst_ref=WB.at[d], send_sem=wx_ss.at[j], recv_sem=wx_rs.at[j],
-            device_id=at((x + NX - j) % NX, y, core), device_id_type=MESH,
+            device_id=at((x - j) & (NX - 1), y, core), device_id_type=MESH,
         )
 
     def wblock(j, s):
-        return (((y + NY - s) % NY) * NX + (x + j) % NX) * 2 + core
+        return (((y - s) & (NY - 1)) * NX + ((x + j) & (NX - 1))) * 2 + core
 
     def wy(j, s, sg):
-        blk = wblock(j, NY - sg * s if not isinstance(s, int) else (-sg * s) % NY)
+        blk = wblock(j, -sg * s)
         return pltpu.make_async_remote_copy(
-            src_ref=WB.at[blk], dst_ref=WB.at[blk], send_sem=wy_ss.at[(sg + 1) // 2, j, s + 1],
-            recv_sem=wy_rs.at[(sg + 1) // 2, j, s + 1],
-            device_id=at(x, (y - sg + NY) % NY, core), device_id_type=MESH,
+            src_ref=WB.at[blk], dst_ref=WB.at[blk], send_sem=wy_ss.at[(sg + 1) >> 1, j, s + 1],
+            recv_sem=wy_rs.at[(sg + 1) >> 1, j, s + 1],
+            device_id=at(x, (y - sg) & (NY - 1), core), device_id_type=MESH,
         )
 
     def wd(blk):
         return pltpu.make_async_remote_copy(
-            src_ref=WB.at[blk], dst_ref=WB.at[blk], send_sem=wd_ss.at[blk // 2], recv_sem=wd_rs.at[blk // 2],
+            src_ref=WB.at[blk], dst_ref=WB.at[blk], send_sem=wd_ss.at[blk >> 1], recv_sem=wd_rs.at[blk >> 1],
             device_id=sib, device_id_type=MESH,
         )
 
@@ -196,7 +198,7 @@
 
     def w_side(j, s, sg, upto):
         most = upto(j, sg)
-        blk = wblock(j, NY - sg * s)
+        blk = wblock(j, -sg * s)
 
         @pl.when(s <= most)
         def _():
@@ -208,11 +210,11 @@
             wy(j, s, sg).start()
 
     def upto(j, sg):
-        even = jnp.where(j % 2 == 0, 1, 0)
+        even = 1 - (j & 1)
         return jnp.where(sg < 0, 3 + even, 4 - even)
 
     def w_tick(i):
-        s, j = i // 4, i % 4
+        s, j = i >> 2, i & 3
 
         @pl.when(s == 0)
         def _():
@@ -261,7 +263,7 @@
 
     def pass1(b):
         for pr in range(2):
-            v = KB[b, :, 128 * pr : 128 * pr + 128].astype(F32)
+            v = KV[b, :, 128 * pr : 128 * pr + 128].astype(F32)
             rt = pltpu.roll(v, 64, 1)
             for o in range(2):
                 dup = jnp.where(lane2 < 64, v, rt) if o == 0 else jnp.where(lane2 < 64, rt, v)
@@ -280,12 +282,13 @@
             E[i, t] = e.reshape(TOK, 256)
 
     def turn_v(b):
-        v = VB[b].astype(F32)
+        v = KV[b + SLOTS].astype(F32)
         i = b - low
         VT[i, :, 0:128] = jnp.transpose(v[0:128]).astype(BF16)
         VT[i, :, 128:256] = jnp.transpose(jnp.concatenate([v[128:192], jnp.zeros((64, 256), F32)], axis=0)).astype(BF16)
 
     def pass2(i):
+        turn_v(i + low)
         for t in range(12):
             g = t // 3
             f = jnp.exp2(MB[i, t] - M[t])
@@ -293,60 +296,84 @@
             OT[t] += jnp.dot(VT[i, 64 * g : 64 * g + 64, 0:TOK], p, preferred_element_type=F32)
 
     pass1(MID)
-    turn_v(MID)
-    late = delay(z)
-
-    def tick(t, carry):
-        def side(j, c2):
-            sg = 1 - 2 * j
-            k_plain = t + 1
-            k_late = t + 1 - late
-            k = jnp.where((sg > 0) | (k_plain <= z), k_plain, k_late)
-            ok = jnp.where(sg > 0, k <= nL, (k <= nR) & ((k_plain <= z) | (k_late > z)))
-
-            @pl.when(ok)
+
+    @pl.when(z == 0)
+    def _():
+        pl.semaphore_wait(late_sem, 1)
+        own(MID, 1)
+
+    def finish():
+        m = M[...]
+        top = jnp.max(m, axis=1, keepdims=True)
+        total = jnp.sum(L[...] * jnp.exp2(m - top), axis=1, keepdims=True)
+        M[...] = jnp.broadcast_to(top + jnp.log(total) * LOG2E, M.shape)
+        pass2(MID - low)
+
+    shift = NC.bit_length() - 1
+    right_up, left_down = pick(N_RIGHT[1:] + N_RIGHT[:1], z), (NZ - 1) - pick(N_RIGHT[-1:] + N_RIGHT[:-1], z)
+
+    def step(_, carry):
+        word, copies, blocks, done = carry
+        digit = word & 7
+        side = digit & 1
+        sg = 2 * side - 1
+        is_copy = digit < 4
+        c_at, b_at = 6 * (digit & 3), 4 * (digit & 3)
+
+        @pl.when(is_copy)
+        def _():
+            n = (copies >> c_at) & 63
+            v = digit >> 1
+            k = (n >> shift) + 1 - v
+            c = n & (NC - 1)
+            b = MID + sg * k + SLOTS * v
+
+            @pl.when(k > 0)
             def _():
-                arrive(KB, ks_sem, kr_sem, sg, k)
-
-                @pl.when(k > LAG)
-                def _():
-                    arrive(VB, vs_sem, vr_sem, sg, k - LAG)
-                    turn_v(MID + sg * (k - LAG))
-
-                pass1(MID + sg * k)
-
-            @pl.when(2 * t + j < WTICKS)
+                kv(b - sg, sg, c).wait_recv()
+
+            @pl.when(k < jnp.where(side == 0, right_up, left_down))
             def _():
-                w_tick(2 * t + j)
-
-            return c2
-
-        return lax.fori_loop(0, 2, side, carry)
-
-    lax.fori_loop(0, TICKS, tick, 0)
-
-    def w_more(i, c):
-        w_tick(i)
-        return c
-
-    lax.fori_loop(2 * TICKS, WTICKS, w_more, 0)
-
-    m = M[...]
-    top = jnp.max(m, axis=1, keepdims=True)
-    total = jnp.sum(L[...] * jnp.exp2(m - top), axis=1, keepdims=True)
-    M[...] = jnp.broadcast_to(top + jnp.log(total) * LOG2E, M.shape)
-
-    for sg, n in ((1, nL), (-1, nR)):
-        for back in range(LAG):
-            k = n - LAG + 1 + back
-            arrive(VB, vs_sem, vr_sem, sg, k)
-            turn_v(MID + sg * k)
-
-    def p2(i, c):
-        pass2(i)
-        return c
-
-    lax.fori_loop(0, NZ, p2, 0)
+                kv(b, sg, c).start()
+
+        n = (blocks >> b_at) & 15
+        b = MID + sg * (n + 1)
+        is_scores = (digit == 4) | (digit == 5)
+
+        @pl.when(is_scores)
+        def _():
+            pass1(b)
+
+            def w(j, c):
+                w_tick(j)
+                return c
+
+            lax.fori_loop((3 * done) >> 1, jnp.minimum((3 * done + 3) >> 1, WTICKS), w, 0)
+
+            @pl.when(done == NZ - 2)
+            def _():
+                finish()
+
+        @pl.when((digit >= 6) & (n < jnp.where(side == 0, nR, nL)))
+        def _():
+            pass2(b - low)
+
+        one = jnp.int32(1)
+        return (
+            word >> 3,
+            copies + jnp.where(is_copy, one << c_at, 0),
+            blocks + jnp.where(is_copy, 0, one << b_at),
+            done + jnp.where(is_scores, 1, 0),
+        )
+
+    def ten(_, carry):
+        words, counts = carry
+        out = lax.fori_loop(0, 10, step, (words[0], *counts))
+        return words[1:] + words[:1], out[1:]
+
+    zero = jnp.int32(0)
+    counts = (jnp.where(z == 0, jnp.int32(NC << 12), 0), zero, zero)
+    lax.fori_loop(0, len(ORDER), ten, (tuple(pick(w, z) for w in ORDER), counts))
 
     for g in range(4):
         for p in range(2):
@@ -375,18 +402,21 @@
         cols = slice(256 * n, 256 * n + 256)
         out_ref[0, :, cols] = (PROJ[n] * r * og_ref[:, cols]).astype(BF16)
 
-    def out_kv(k, c):
-        for sg in (-1, 1):
-            sent(KB, ks_sem, kr_sem, sg, k)
-            sent(VB, vs_sem, vr_sem, sg, k)
-        return c
-
-    lax.fori_loop(0, 10, out_kv, 0)
+    for sg, most in ((-1, right_up), (1, left_down)):
+
+        def gone(k, carry):
+            for c in range(NC):
+                kv(MID + sg * k, sg, c).wait_send()
+                kv(MID + SLOTS + sg * k, sg, c).wait_send()
+            return carry
+
+        lax.fori_loop(0, most, gone, 0)
+
     for j in (1, 2, 3):
         wx(j).wait_send()
 
     def out_w(i, c):
-        s, j = i // 4, i % 4
+        s, j = i >> 2, i & 3
         for sg in (-1, 1):
 
             @pl.when(s + 1 <= upto(j, sg))
@@ -415,22 +445,22 @@
         in_specs=[hbm, hbm, hbm, hbm, vmem, vmem, vmem, hbm, hbm, hbm],
         out_specs=vmem,
         scratch_shapes=[
-            pltpu.VMEM((TOK, 1024), BF16), pltpu.VMEM((TOK, 256), BF16), pltpu.VMEM((1024, 32), BF16),
+            pltpu.VMEM((TOK, 1024), BF16), pltpu.VMEM((TOK, 256), BF16),
             pltpu.VMEM((2, 8, 256), F32), pltpu.VMEM((2, 64, 256), F32), pltpu.VMEM((2, 256, 256), BF16),
-            pltpu.VMEM((SLOTS, TOK, 256), BF16), pltpu.VMEM((SLOTS, TOK, 256), BF16), pltpu.VMEM((NZ, 256, 256), BF16),
+            pltpu.VMEM((2 * SLOTS, TOK, 256), BF16), pltpu.VMEM((NZ, 256, 256), BF16),
             pltpu.VMEM((64, 32, 1024), BF16), pltpu.VMEM((12, 256, 256), BF16), pltpu.VMEM((4, TOK, 256), BF16),
             pltpu.VMEM((12, 8, 256), F32), pltpu.VMEM((12, 8, 256), F32), pltpu.VMEM((NZ, 12, 8, 256), F32),
             pltpu.VMEM((NZ, 12, TOK, 256), F32), pltpu.VMEM((12, 64, 256), F32), pltpu.VMEM((TOK, 1024), BF16),
             pltpu.VMEM((8, TOK, 256), F32),
-            dma((7,)), dma((SLOTS, NC)), dma((SLOTS, NC)), dma((SLOTS, NC)), dma((SLOTS, NC)),
-            dma((4,)), dma((4,)), dma((2, 4, 5)), dma((2, 4, 5)), dma((32,)), dma((32,)),
+            dma((7,)), dma((2 * SLOTS, NC)), dma((2 * SLOTS, NC)),
+            dma((4,)), dma((4,)), dma((2, 4, 5)), dma((2, 4, 5)), dma((32,)), dma((32,)), pltpu.SemaphoreType.REGULAR,
         ],
         compiler_params=pltpu.CompilerParams(
             collective_id=0, has_side_effects=True, vmem_limit_bytes=67043328
         ),
         name="attend",
     )(
-        queries, keys, values, out_weight, query_gain[None], key_gain[None], out_gain[None],
+        queries, keys, values, out_weight.T, query_gain[None], key_gain[None], out_gain[None],
         jnp.asarray(row_tab), jnp.asarray(col_tab), jnp.asarray(mats),
     )
 

time: 90.9 us -> 71.6 us (0.79)
  the two profiles are of different devices: /device:TPU:272 before, /device:TPU:24 now
where the time goes in v2:
time: 71.6 us; the launch traced here: 71.3 us
  Pallas kernels  69.2 us (97%)
  local copies, waits for them, and re-layouts  2.09 us (3%)
    pallas_call x1, Pallas kernels, per_device(): pl.pallas_call(kernel, out_shape=jax.ShapeDtypeStruct((1, TOK, 2048), BF1...  69.2 us
    unnamed x1, local copies, waits for them, and re-layouts  2.09 us

profile of v2, /device:TPU:24, one launch (start us, length us, event | category | flops | bytes accessed | tf_op | source)
XLA Modules:
  0.0 71.3 jit_solution(17290310708924821107)
XLA Ops:
  0.0 69.2 %attend.1 = bf16[1,192,2048]{2,1,0:T(8,128)(2,1)} custom-call(bf16[1,192,1024]{2,1,0:T(8,128)(2,1)} %q_hbm.1, bf16[1,192,256]{2,1,0:T(8,128)(2,1)} %k_hbm.1, bf16[1,192,256]{2,1,0:T(8,128)(2,1)} %v_hbm.1, bf16[32,1024]{1,0:T(8,128)(2,1)} %bitcast.4, f32[1,64]{1,0:T(1,128)} %bitcast.6, f32[1,64]{1,0:T(1,128)} %bitcast.7, f32[1,2048]{1,0:T(1,128)} %bitcast.5, ...), custom_call_target="tpu_custom_call" | custom-call | tf_op jit(solution)/shard_map/attend/pallas_call | solution.py:442
  69.2 2.1 %copy.12 = bf16[1,192,2048]{2,1,0:T(8,128)(2,1)} copy(bf16[1,192,2048]{2,1,0:T(8,128)(2,1)} %attend.1) | data formatting | bytes 1572864

commit v3 on v2

--- a/solution.py
+++ b/solution.py
@@ -19,20 +19,46 @@
 EPS = 1e-06
 MID = 10
 SLOTS = 21
-NC = 2
+NC = 4
 WTICKS = 20
-N_RIGHT = (7, 7, 7, 7, 7, 7, 7, 7, 7, 7, 7, 7, 7, 7, 7, 7)
+N_RIGHT = (7, 7, 7, 7, 7, 7, 7, 7, 8, 8, 8, 8, 8, 8, 8, 7)
 ORDER = (
-    (328470619, 293635227, 170919067, 293635227, 293635227, 696288411, 176424091, 293635227, 621024411, 621024411, 621024411, 621024411, 621024411, 621024411, 621024411, 696288411),
-    (327320203, 192190165, 290326058, 170930389, 170930389, 170930386, 170930389, 170930389, 696288922, 696288922, 696288922, 696288922, 696288922, 696288922, 696288915, 621024467),
-    (327320203, 696289001, 192190185, 290326058, 290326058, 290326058, 290326058, 170930410, 696288922, 696288922, 696288922, 696288922, 696288922, 696288922, 696288915, 621024467),
-    (327323731, 696288922, 290308137, 410293993, 174702913, 174702913, 290326337, 170930410, 696288922, 696288922, 696288922, 696288922, 696288922, 696288922, 696288915, 621024467),
-    (327323731, 170930386, 172867625, 409637984, 547624681, 172898824, 290326337, 170930410, 696288922, 696288922, 696288922, 696288922, 696288922, 696288922, 696288915, 621024467),
-    (327323731, 290326037, 174702920, 409555552, 51684051, 696289001, 290326337, 170930410, 696288922, 696288922, 696288922, 696288922, 696288922, 696288922, 696288915, 621024467),
-    (694325913, 290326057, 40487432, 409637984, 409637980, 547624147, 691024105, 290326338, 170930330, 696288922, 696288922, 696288922, 696288922, 696288922, 696288915, 621024467),
-    (1055471384, 376029505, 860705537, 508469856, 510301280, 1047831195, 1047828122, 1047828201, 1047828181, 1047828122, 1047828122, 1047828122, 1047828122, 1047828122, 1047828115, 930387155),
-    (1056698302, 937393663, 937394167, 1056701943, 1056931319, 1071611379, 937393651, 937393651, 937393651, 937393651, 937393651, 937393651, 937393651, 937393651, 937393651, 1056698299),
-    (920350135, 920350199, 920350647, 920350654, 920350654, 920350654, 920350711, 920350711, 920350711, 920350711, 920350711, 920350711, 920350711, 920350711, 920350711, 920350654),
+    (
+        (18895433, 6391506, 6391506, 543262416, 6391506, 6391506, 6391506, 799899, 537670683, 135083163, 135083163, 865435, 139277467, 135083163, 21836955, 5059739),
+        (304521985, 692393044, 136348308, 201592850, 688133188, 688133260, 673227404, 17044628, 10818641, 446961672, 329586696, 489202433, 491127304, 329826824, 576884801, 692623368),
+        (409045585, 153466578, 443369093, 409051466, 55412944, 55412760, 55588056, 56763945, 290326043, 293701146, 16877210, 17576146, 136414867, 136414874, 16790739, 86016657),
+        (289743584, 690271965, 690267282, 172270872, 692328456, 692099080, 2490882, 36045443, 51675665, 51675793, 320118860, 413475468, 441357408, 329881610, 305439372, 220795649),
+        (543262249, 136349403, 488937179, 443102538, 325714128, 444696216, 454046761, 543262377, 136423108, 36255939, 306561219, 25265690, 539002394, 201360922, 170037313, 413405250),
+        (688198795, 323834976, 413438683, 463770266, 289711187, 159417408, 201597592, 692326593, 313268234, 73568321, 543330369, 543330385, 409588817, 285643858, 172401248, 21836956),
+        (309200408, 335810755, 174702784, 460624475, 308917461, 443102378, 51217738, 409052440, 176195099, 201601242, 136393939, 21312723, 137363994, 293884424, 470569480, 407801921),
+        (413406289, 51194449, 51675786, 176164875, 460231249, 155755162, 170439937, 692633672, 336351752, 403526273, 279713800, 327944769, 203456842, 21254794, 169911962, 136881820),
+        (304481944, 289980611, 304719619, 51197258, 50451017, 424490218, 323827349, 23168666, 17118419, 17118880, 270927387, 136320211, 136911442, 319916609, 443646280, 443648520),
+        (409045585, 543263297, 580944385, 289980483, 287941379, 158186057, 491066449, 447030017, 445221441, 313333761, 543263313, 35934304, 156242248, 176197827, 17109202, 136872602),
+        (189081312, 2692314, 140608723, 50431657, 6391465, 470569032, 153957586, 304719514, 202122768, 17051803, 136348890, 173310721, 409741130, 57255145, 407750185, 309208616),
+        (489428611, 324031105, 354985056, 692393164, 692396643, 21304979, 136427241, 443192401, 329818769, 458052684, 170218592, 844106305, 543228160, 409544704, 441264128, 488902736),
+        (443136003, 16811731, 52965571, 327266328, 544047130, 326109000, 309663808, 690271442, 304428243, 172528730, 317402442, 988411635, 1073293211, 516554968, 373948440, 466560736),
+        (869121178, 860705364, 458531916, 329585290, 866456657, 488969306, 488937115, 891590363, 508406353, 986393749, 443266238, 323856274, 307084442, 318584286, 528349086, 508116638),
+        (937373691, 1046461850, 1073309598, 1073440499, 1073424094, 1073429747, 1073440499, 1073428379, 1073423763, 460318162, 460268691, 460924562, 508114138, 317564571, 306951898, 460177147),
+        (937393655, 937393655, 937393655, 937393655, 937393655, 937393655, 937393655, 937393655, 937393655, 937393655, 937393655, 937393655, 937393655, 937393654, 937393654, 937393655),
+    ),
+    (
+        (135561737, 341935808, 73500352, 411141824, 73500352, 73500352, 207718080, 543261912, 159483584, 17051803, 17051803, 23081115, 17138843, 21246107, 17044635, 135017627),
+        (18129996, 312808529, 692453896, 136364096, 674238529, 411308097, 403997248, 137367616, 403998288, 56787468, 56795788, 404005516, 442671873, 325231361, 56764225, 145039968),
+        (491569217, 153466011, 309143250, 323831301, 189890776, 288372229, 310478532, 56755752, 539002564, 136357572, 134529219, 170442947, 293634755, 674238529, 171016282, 18121226),
+        (17052866, 690271965, 354751626, 707306123, 404005514, 51204746, 413406289, 292160009, 543951425, 453161056, 411840840, 588087624, 137113937, 51131547, 136938312, 135569932),
+        (55332940, 151262939, 488937179, 174666970, 170442947, 170526235, 170505472, 170501845, 136877274, 688202336, 137367635, 201593368, 51684448, 220243020, 288690440, 437552204),
+        (136386307, 325715485, 86020827, 457872458, 323857034, 6312586, 453154314, 51139082, 189806085, 424773144, 458241541, 17147432, 141312195, 711331904, 201621834, 169984195),
+        (57770314, 413405249, 170922203, 409899595, 289739987, 289711828, 289740448, 170436308, 441754250, 84255370, 84218506, 409117324, 27531272, 201593347, 55413258, 56644234),
+        (17080986, 21247650, 453783889, 159417027, 191440553, 443372627, 543273001, 202125640, 17044691, 323356187, 289800731, 170739224, 458494474, 17077418, 17044760, 169903828),
+        (203726953, 411830849, 285553760, 140608746, 51687944, 86549130, 692393050, 86550161, 441819907, 174756945, 409056425, 19038858, 151262292, 425854661, 325666345, 458334536),
+        (728340993, 189825235, 411141673, 86614785, 136648348, 23670995, 271099602, 293875907, 688132179, 413406298, 289740824, 325755649, 354762821, 355074568, 539001475, 176195200),
+        (309212675, 57168392, 202146881, 201601235, 443560168, 447030024, 55877715, 458532490, 439355016, 407742488, 285775017, 335815176, 6398163, 409481347, 543262529, 153430609),
+        (527034014, 21304516, 291602666, 51204616, 486842442, 192975040, 290039554, 170435226, 329816080, 337675330, 336344385, 376267945, 451782036, 466332820, 986426515, 978270109),
+        (460928250, 459931979, 447025824, 692360916, 156014336, 158148426, 458135114, 174626005, 325793178, 995714217, 468429974, 451653338, 323727006, 306804383, 393033362, 309964499),
+        (458041307, 392953526, 1070316787, 995833235, 987358933, 868858457, 913216081, 510601034, 986296023, 317402778, 307836567, 307177114, 307836115, 325662098, 323599507, 459125971),
+        (936977559, 306783410, 306783706, 306951871, 317566651, 528039894, 528349086, 469628830, 392799378, 317535450, 392770771, 392799450, 466199762, 508404891, 392799450, 460269203),
+        (937393655, 937393654, 937393654, 937393654, 937393654, 937393655, 937393655, 937393655, 937393654, 937393654, 937393654, 937393654, 937393655, 937393655, 937393654, 937393655),
+    ),
 )
 
 
@@ -91,9 +117,9 @@
 
 
 def kernel(
-    q_hbm, k_hbm, v_hbm, w_hbm, qg_ref, kg_ref, og_ref, row_hbm, col_hbm, mats_hbm,
+    q_hbm, k_hbm, v_hbm, w_hbm, qg_hbm, kg_hbm, og_hbm, row_hbm, col_hbm, mats_hbm,
     out_ref,
-    qb, kraw, row_tab, col_tab, mats,
+    qb, kraw, row_tab, col_tab, mats, qg_ref, kg_ref, og_ref,
     KV, VT, WB, QX, KX, M, L, MB, E, OT, ATT, PROJ,
     in_sem, s_sem, r_sem, wx_ss, wx_rs, wy_ss, wy_rs, wd_ss, wd_rs, late_sem,
 ):
@@ -113,9 +139,12 @@
         pltpu.make_async_copy(row_hbm.at[z], row_tab, in_sem.at[1]),
         pltpu.make_async_copy(col_hbm, col_tab, in_sem.at[2]),
         pltpu.make_async_copy(mats_hbm, mats, in_sem.at[3]),
+        pltpu.make_async_copy(kg_hbm, kg_ref, in_sem.at[7]),
         pltpu.make_async_copy(v_hbm.at[0], KV.at[MID + SLOTS], in_sem.at[4]),
         pltpu.make_async_copy(w_hbm, WB.at[d], in_sem.at[5]),
         pltpu.make_async_copy(q_hbm.at[0], qb, in_sem.at[6]),
+        pltpu.make_async_copy(qg_hbm, qg_ref, in_sem.at[8]),
+        pltpu.make_async_copy(og_hbm, og_ref, in_sem.at[9]),
     ]
     for c in loads:
         c.start()
@@ -134,12 +163,12 @@
     def _():
         pl.semaphore_signal(barrier, inc=1, device_id=(up, d), device_id_type=MESH)
 
-    for c in loads[:4]:
+    for c in loads[:5]:
         c.wait()
     kg = gain_rows(kg_ref[...])
     KV[MID] = rope(kraw[...], kg, row_tab, col_tab, mats).astype(BF16)
-    loads[4].wait()
     loads[5].wait()
+    loads[6].wait()
     pl.semaphore_wait(barrier, len(partners) + jnp.where(z == 0, 0, 1))
 
     @pl.when(z == NZ - 1)
@@ -151,7 +180,7 @@
     def kv(b, sg, c):
         rows = pl.ds(c * (TOK // NC), TOK // NC)
         return pltpu.make_async_remote_copy(
-            src_ref=KV.at[b, rows], dst_ref=KV.at[b + sg, rows], send_sem=s_sem.at[b + sg, c],
+            src_ref=KV.at[b, rows], dst_ref=KV.at[b + sg, rows], send_sem=s_sem.at[(sg + 1) >> 1],
             recv_sem=r_sem.at[b + sg, c], device_id=(there(sg), d), device_id_type=MESH,
         )
 
@@ -171,7 +200,7 @@
 
     def wx(j):
         return pltpu.make_async_remote_copy(
-            src_ref=WB.at[d], dst_ref=WB.at[d], send_sem=wx_ss.at[j], recv_sem=wx_rs.at[j],
+            src_ref=WB.at[d], dst_ref=WB.at[d], send_sem=wx_ss, recv_sem=wx_rs.at[j],
             device_id=at((x - j) & (NX - 1), y, core), device_id_type=MESH,
         )
 
@@ -181,14 +210,14 @@
     def wy(j, s, sg):
         blk = wblock(j, -sg * s)
         return pltpu.make_async_remote_copy(
-            src_ref=WB.at[blk], dst_ref=WB.at[blk], send_sem=wy_ss.at[(sg + 1) >> 1, j, s + 1],
+            src_ref=WB.at[blk], dst_ref=WB.at[blk], send_sem=wy_ss,
             recv_sem=wy_rs.at[(sg + 1) >> 1, j, s + 1],
             device_id=at(x, (y - sg) & (NY - 1), core), device_id_type=MESH,
         )
 
     def wd(blk):
         return pltpu.make_async_remote_copy(
-            src_ref=WB.at[blk], dst_ref=WB.at[blk], send_sem=wd_ss.at[blk >> 1], recv_sem=wd_rs.at[blk >> 1],
+            src_ref=WB.at[blk], dst_ref=WB.at[blk], send_sem=wd_ss, recv_sem=wd_rs,
             device_id=sib, device_id_type=MESH,
         )
 
@@ -231,7 +260,8 @@
             w_side(j, s, -1, upto)
             w_side(j, s, 1, upto)
 
-    loads[6].wait()
+    for c in loads[7:]:
+        c.wait()
     qg = gain_rows(qg_ref[...])
     lane = lax.broadcasted_iota(jnp.int32, (64, 128), 1)
 
@@ -281,19 +311,17 @@
             MB[i, t] = new
             E[i, t] = e.reshape(TOK, 256)
 
-    def turn_v(b):
-        v = KV[b + SLOTS].astype(F32)
-        i = b - low
-        VT[i, :, 0:128] = jnp.transpose(v[0:128]).astype(BF16)
-        VT[i, :, 128:256] = jnp.transpose(jnp.concatenate([v[128:192], jnp.zeros((64, 256), F32)], axis=0)).astype(BF16)
-
-    def pass2(i):
-        turn_v(i + low)
+    def pass2(m):
+        v = KV[pl.ds(SLOTS + low + 2 * m, 2)].reshape(2 * TOK, 256)
+        for c in range(3):
+            VT[:, 128 * c : 128 * c + 128] = jnp.transpose(v[128 * c : 128 * c + 128].astype(F32)).astype(BF16)
         for t in range(12):
             g = t // 3
-            f = jnp.exp2(MB[i, t] - M[t])
-            p = (E[i, t].reshape(TOK // 8, 8, 256) * f[None]).reshape(TOK, 256).astype(BF16)
-            OT[t] += jnp.dot(VT[i, 64 * g : 64 * g + 64, 0:TOK], p, preferred_element_type=F32)
+            p = []
+            for i in (2 * m, 2 * m + 1):
+                f = jnp.exp2(MB[i, t] - M[t])
+                p.append((E[i, t].reshape(TOK // 8, 8, 256) * f[None]).reshape(TOK, 256).astype(BF16))
+            OT[t] += jnp.dot(VT[64 * g : 64 * g + 64], jnp.concatenate(p, axis=0), preferred_element_type=F32)
 
     pass1(MID)
 
@@ -307,7 +335,6 @@
         top = jnp.max(m, axis=1, keepdims=True)
         total = jnp.sum(L[...] * jnp.exp2(m - top), axis=1, keepdims=True)
         M[...] = jnp.broadcast_to(top + jnp.log(total) * LOG2E, M.shape)
-        pass2(MID - low)
 
     shift = NC.bit_length() - 1
     right_up, left_down = pick(N_RIGHT[1:] + N_RIGHT[:1], z), (NZ - 1) - pick(N_RIGHT[-1:] + N_RIGHT[:-1], z)
@@ -354,9 +381,9 @@
             def _():
                 finish()
 
-        @pl.when((digit >= 6) & (n < jnp.where(side == 0, nR, nL)))
-        def _():
-            pass2(b - low)
+        @pl.when((digit >= 6) & (n < 4))
+        def _():
+            pass2(jnp.where(side == 0, 3 - n, 4 + n))
 
         one = jnp.int32(1)
         return (
@@ -373,7 +400,8 @@
 
     zero = jnp.int32(0)
     counts = (jnp.where(z == 0, jnp.int32(NC << 12), 0), zero, zero)
-    lax.fori_loop(0, len(ORDER), ten, (tuple(pick(w, z) for w in ORDER), counts))
+    words = tuple(jnp.where(core == 0, pick(a, z), pick(b, z)) for a, b in zip(*ORDER))
+    lax.fori_loop(0, len(words), ten, (words, counts))
 
     for g in range(4):
         for p in range(2):
@@ -383,80 +411,63 @@
             b = jnp.transpose(jnp.concatenate([b, b], axis=0))
             ATT[128:192, 256 * g + 128 * p : 256 * g + 128 * p + 128] = jnp.where(lane < 64, b[0:64], b[64:128]).astype(BF16)
 
-    def w_in(i, c):
-        wd(2 * i + 1 - core).wait_recv()
-        return c
-
-    lax.fori_loop(0, NX * NY, w_in, 0)
-
-    def project(n, ss):
-        w = WB[pl.ds(8 * n, 8)].reshape(256, 1024)
-        pr = lax.dot_general(ATT[...], w, (((1,), (1,)), ((), ())), preferred_element_type=F32)
-        PROJ[n] = pr
-        sq = pr * pr
-        return ss + sq[:, 0:128] + sq[:, 128:256]
-
-    ss = lax.fori_loop(0, 8, project, jnp.zeros((TOK, 128), F32))
+    def all_w(n, ss, rs):
+        part = WB.at[pl.ds(0, n)]
+        return pltpu.make_async_remote_copy(
+            src_ref=part, dst_ref=part, send_sem=ss, recv_sem=rs, device_id=sib, device_id_type=MESH
+        )
+
+    all_w(NX * NY, wd_ss, wd_rs).wait_recv()
+
+    w = WB[...].reshape(2048, 1024)
+    pr = lax.dot_general(ATT[...], w, (((1,), (1,)), ((), ())), preferred_element_type=F32)
+    PROJ[...] = pr
+    sq = pr * pr
+    ss = sum(sq[:, 128 * c : 128 * c + 128] for c in range(16))
     r = lax.rsqrt(jnp.sum(ss, axis=1, keepdims=True) / 2048.0 + EPS)
-    for n in range(8):
-        cols = slice(256 * n, 256 * n + 256)
-        out_ref[0, :, cols] = (PROJ[n] * r * og_ref[:, cols]).astype(BF16)
-
-    for sg, most in ((-1, right_up), (1, left_down)):
-
-        def gone(k, carry):
-            for c in range(NC):
-                kv(MID + sg * k, sg, c).wait_send()
-                kv(MID + SLOTS + sg * k, sg, c).wait_send()
-            return carry
-
-        lax.fori_loop(0, most, gone, 0)
-
-    for j in (1, 2, 3):
-        wx(j).wait_send()
-
-    def out_w(i, c):
-        s, j = i >> 2, i & 3
-        for sg in (-1, 1):
-
-            @pl.when(s + 1 <= upto(j, sg))
+    for i in range(3):
+        rows = slice(64 * i, 64 * i + 64)
+        out_ref[0, rows] = (PROJ[rows] * r[rows] * og_ref[...]).astype(BF16)
+
+    for side, n, values in ((0, right_up, set(N_RIGHT)), (1, left_down, {NZ - 1 - v for v in N_RIGHT})):
+        for v in sorted(values):
+
+            @pl.when(n == v)
             def _():
-                wy(j, s, sg).wait_send()
-
-        return c
-
-    lax.fori_loop(0, 16, out_w, 0)
-
-    def out_d(i, c):
-        wd(2 * i + core).wait_send()
-        return c
-
-    lax.fori_loop(0, NX * NY, out_d, 0)
+                part = KV.at[pl.ds(0, 2 * v)]
+                pltpu.make_async_remote_copy(
+                    src_ref=part, dst_ref=part, send_sem=s_sem.at[side], recv_sem=s_sem.at[side],
+                    device_id=(up, d), device_id_type=MESH,
+                ).wait_send()
+
+    all_w(3, wx_ss, wd_rs).wait_send()
+    all_w(28, wy_ss, wd_rs).wait_send()
+    all_w(NX * NY, wd_ss, wd_rs).wait_send()
 
 
 def per_device(queries, keys, values, query_gain, key_gain, out_weight, out_gain):
     row_tab, col_tab, mats = tables()
     hbm = pl.BlockSpec(memory_space=pl.ANY)
-    vmem = pl.BlockSpec(memory_space=pltpu.VMEM)
     dma = pltpu.SemaphoreType.DMA
     return pl.pallas_call(
         kernel,
-        out_shape=jax.ShapeDtypeStruct((1, TOK, 2048), BF16),
-        in_specs=[hbm, hbm, hbm, hbm, vmem, vmem, vmem, hbm, hbm, hbm],
-        out_specs=vmem,
+        out_shape=pltpu.VMEM((1, TOK, 2048), BF16),
+        in_specs=[hbm] * 10,
+        out_specs=pl.BlockSpec(memory_space=pltpu.VMEM),
         scratch_shapes=[
             pltpu.VMEM((TOK, 1024), BF16), pltpu.VMEM((TOK, 256), BF16),
             pltpu.VMEM((2, 8, 256), F32), pltpu.VMEM((2, 64, 256), F32), pltpu.VMEM((2, 256, 256), BF16),
-            pltpu.VMEM((2 * SLOTS, TOK, 256), BF16), pltpu.VMEM((NZ, 256, 256), BF16),
+            pltpu.VMEM((1, 64), F32), pltpu.VMEM((1, 64), F32), pltpu.VMEM((1, 2048), F32),
+            pltpu.VMEM((2 * SLOTS, TOK, 256), BF16), pltpu.VMEM((256, 2 * TOK), BF16),
             pltpu.VMEM((64, 32, 1024), BF16), pltpu.VMEM((12, 256, 256), BF16), pltpu.VMEM((4, TOK, 256), BF16),
             pltpu.VMEM((12, 8, 256), F32), pltpu.VMEM((12, 8, 256), F32), pltpu.VMEM((NZ, 12, 8, 256), F32),
             pltpu.VMEM((NZ, 12, TOK, 256), F32), pltpu.VMEM((12, 64, 256), F32), pltpu.VMEM((TOK, 1024), BF16),
-            pltpu.VMEM((8, TOK, 256), F32),
-            dma((7,)), dma((2 * SLOTS, NC)), dma((2 * SLOTS, NC)),
-            dma((4,)), dma((4,)), dma((2, 4, 5)), dma((2, 4, 5)), dma((32,)), dma((32,)), pltpu.SemaphoreType.REGULAR,
+            pltpu.VMEM((TOK, 2048), F32),
+            dma((10,)), dma((2,)), dma((2 * SLOTS, NC)),
+            dma, dma((4,)), dma, dma((2, 4, 5)), dma, dma, pltpu.SemaphoreType.REGULAR,
         ],
         compiler_params=pltpu.CompilerParams(
-            collective_id=0, has_side_effects=True, vmem_limit_bytes=67043328
+            collective_id=0, has_side_effects=True, vmem_limit_bytes=58000000
         ),
         name="attend",
     )(

time: 71.6 us -> 65.2 us (0.911)
  the two profiles are of different devices: /device:TPU:24 before, /device:TPU:1 now
where the time goes in v3:
time: 65.2 us; the launch traced here: 65 us
  Pallas kernels  64.1 us (98%)
  local copies, waits for them, and re-layouts  0.88 us (1%)
    pallas_call x1, Pallas kernels, per_device(): pl.pallas_call(kernel, out_shape=pltpu.VMEM((1, TOK, 2048), BF16), in_spe...  64.1 us

profile of v3, /device:TPU:1, one launch (start us, length us, event | category | flops | bytes accessed | tf_op | source)
XLA Modules:
  0.0 65.0 jit_solution(9139060901049419780)
XLA Ops:
  0.0 64.1 %attend.1 = bf16[1,192,2048]{2,1,0:T(8,128)(2,1)S(1)} custom-call(bf16[1,192,1024]{2,1,0:T(8,128)(2,1)} %q_hbm.1, bf16[1,192,256]{2,1,0:T(8,128)(2,1)} %k_hbm.1, bf16[1,192,256]{2,1,0:T(8,128)(2,1)} %v_hbm.1, bf16[32,1024]{1,0:T(8,128)(2,1)} %bitcast.4, f32[1,64]{1,0:T(1,128)} %bitcast.6, f32[1,64]{1,0:T(1,128)} %bitcast.7, f32[1,2048]{1,0:T(1,128)} %bitcast.5, ...), custom_call_target="tpu_custom_call" | custom-call | tf_op jit(solution)/shard_map/attend/pallas_call | solution.py:452
  64.2 0.9 %copy.12 = bf16[1,192,2048]{2,1,0:T(8,128)(2,1)} copy(bf16[1,192,2048]{2,1,0:T(8,128)(2,1)S(1)} %attend.1) | data formatting | bytes 1572864
